TPU v7x, 32 devices: a whole 2x2x4 slice. The times are simulated.
32 devices in a mesh: sp: 8 (over z, y), tp: 4 (over x, core).
Axes of the slice: x: 2, y: 2, z: 4, core: 2. Of those that a mesh axis runs over, the one named last changes fastest.
Arguments:
- tokens: bfloat16 [3072, 4096], P(('sp', 'tp')), may hold values from -6 to 6
- norm_gain: float32 [4096], replicated, may hold values from 0.1 to 1.9
- w_query: bfloat16 [4096, 2048], P('sp', 'tp'), may hold values from -0.09375 to 0.09375
- w_key: bfloat16 [4096, 512], P('sp', 'tp'), may hold values from -1.5 to 1.5
- w_value: bfloat16 [4096, 512], P('sp', 'tp'), may hold values from -0.09375 to 0.09375
- w_mem_query: bfloat16 [4096, 1024], P('sp', 'tp'), may hold values from -0.09375 to 0.09375
- w_mem_key: bfloat16 [4096, 1024], P('sp', 'tp'), may hold values from -0.09375 to 0.09375
- w_mem_value: bfloat16 [4096, 1024], P('sp', 'tp'), may hold values from -0.09375 to 0.09375
- w_mem_gate: bfloat16 [4096, 1024], P('sp', 'tp'), may hold values from -0.09375 to 0.09375
- w_gates: bfloat16 [4096, 2, 16], replicated, may hold values from -0.09375 to 0.09375
- sinks: float32 [32], P('tp'), may hold values from 2 to 6
- forget_bias: float32 [16], P('tp'), may hold values from 3 to 13
- forget_shift: float32 [3072, 16], P('sp', 'tp'), may hold values from -1 to 0
- w_out: bfloat16 [3072, 4096], P('sp', 'tp'), may hold values from -0.21650635 to 0.21650635
Outputs:
- mixed: bfloat16 [3072, 4096], P('sp', 'tp')
- log_total: float32 [3072, 32], P('sp', 'tp')
All inputs are finite; a program needn't handle non-finite values.
Results may differ from a plain program's by a relative error of at most 0.018.
Values may be sent and summed in bfloat16 or wider, within the bound.
A program may use at most 128 MiB of HBM per device.

v0:
```python
import math
import jax
import jax.numpy as jnp
from jax import lax
from jax.sharding import PartitionSpec as P

HD = 64
WINDOW = 128
BLK = 128
EPSILON = 1e-06
MASKED = -1e30
exact_precision = lax.Precision.HIGHEST


def passed_along(block, axis, distance):
    devices = range(lax.axis_size(axis))
    route = [(i - distance, i) for i in devices if i - distance in devices]
    return lax.ppermute(block, axis, route)


def entering(x, axis, join, neutral):
    place = lax.axis_index(axis)
    gathered = jax.tree.map(
        lambda a, kind: lax.all_gather(a.astype(kind), axis),
        x,
        (jnp.bfloat16, jnp.bfloat16, jnp.bfloat16, jnp.bfloat16),
    )
    state = jax.tree.map(lambda a, e: jnp.zeros_like(a) + jnp.asarray(e, a.dtype), x, neutral)

    def one(turn, state):
        return join(
            state,
            jax.tree.map(
                lambda a, own: lax.dynamic_index_in_dim(a, turn, 0, False).astype(own.dtype),
                gathered,
                x,
            ),
        )

    return lax.fori_loop(0, place, one, state)


def normalize(tokens, norm_gain):
    values = tokens.astype(jnp.float32)
    rescale = lax.rsqrt(jnp.mean(values * values, axis=-1, keepdims=True) + EPSILON)
    return (values * rescale * norm_gain).astype(jnp.bfloat16)


def advance(carried, key_block, value_block, in_block, cumulative):
    memory_state, normalizer, stabilizer = carried
    block_total = cumulative[:, -1]
    decays = block_total[:, None] - cumulative + in_block
    new_stabilizer = jnp.maximum(block_total + stabilizer, jnp.max(decays, axis=-1))
    weights = jnp.exp(decays - new_stabilizer[:, None])
    rescale = jnp.exp(block_total + stabilizer - new_stabilizer)
    new_state = rescale[:, None, None] * memory_state + jnp.einsum(
        "hsv,hsk->hvk", value_block * weights[:, :, None], key_block, precision=exact_precision
    )
    new_normalizer = rescale[:, None] * normalizer + jnp.einsum(
        "hs,hsk->hk", weights, key_block, precision=exact_precision
    )
    return (new_state, new_normalizer, new_stabilizer)


def block_step(carried, block_data):
    memory_state, normalizer, stabilizer = carried
    query_block, key_block, value_block, in_block, forget_block = block_data
    length = in_block.shape[-1]
    cumulative = jnp.cumsum(forget_block, axis=-1)
    causal = lax.broadcasted_iota(jnp.int32, (length, length), 0) >= lax.broadcasted_iota(
        jnp.int32, (length, length), 1
    )
    log_weight = jnp.where(
        causal[None], cumulative[:, :, None] - cumulative[:, None, :] + in_block[:, None, :], MASKED
    )
    row_level = jnp.maximum(cumulative + stabilizer[:, None], jnp.max(log_weight, axis=-1))
    carried_part = jnp.exp(cumulative + stabilizer[:, None] - row_level)
    affinity = jnp.einsum(
        "htd,hsd->hts", query_block, key_block, precision=exact_precision
    ) * jnp.exp(log_weight - row_level[:, :, None])
    numerator = carried_part[:, :, None] * jnp.einsum(
        "hvk,htk->htv", memory_state, query_block, precision=exact_precision
    ) + jnp.einsum("hts,hsv->htv", affinity, value_block, precision=exact_precision)
    denominator = carried_part * jnp.einsum(
        "hk,htk->ht", normalizer, query_block, precision=exact_precision
    ) + jnp.sum(affinity, axis=-1)
    recall = numerator / jnp.maximum(jnp.abs(denominator), jnp.exp(-row_level))[:, :, None]
    return (advance(carried, key_block, value_block, in_block, cumulative), recall)


def join_states(earlier, later):
    passed_one, state_one, normal_one, level_one = earlier
    passed_two, state_two, normal_two, level_two = later
    new_level = jnp.maximum(passed_two + level_one, level_two)
    weight_one = jnp.exp(passed_two + level_one - new_level)
    weight_two = jnp.exp(level_two - new_level)
    new_state = weight_one[:, None, None] * state_one + weight_two[:, None, None] * state_two
    new_normal = weight_one[:, None] * normal_one + weight_two[:, None] * normal_two
    return (passed_one + passed_two, new_state, new_normal, new_level)


def attend(query, key_rows, value_rows, sinks):
    row_count = query.shape[0]
    kv_local = key_rows.shape[1] // HD
    group_size = query.shape[1] // HD // kv_local
    block_count = row_count // WINDOW
    rim_key, rim_value = passed_along(
        (key_rows[row_count - WINDOW :], value_rows[row_count - WINDOW :]), "sp", 1
    )
    padded_keys = jnp.concatenate([rim_key, key_rows], axis=0).reshape(
        block_count + 1, WINDOW, kv_local, HD
    )
    padded_values = jnp.concatenate([rim_value, value_rows], axis=0).reshape(
        block_count + 1, WINDOW, kv_local, HD
    )
    key_window = jnp.concatenate([padded_keys[:-1], padded_keys[1:]], axis=1)
    value_window = jnp.concatenate([padded_values[:-1], padded_values[1:]], axis=1)
    q_blocks = query.reshape(block_count, WINDOW, kv_local, group_size, HD)
    scores = jnp.einsum(
        "nqhgd,nkhd->nhgqk", q_blocks, key_window, preferred_element_type=jnp.float32
    ) * HD ** (-0.5)
    query_index = lax.broadcasted_iota(jnp.int32, (WINDOW, 2 * WINDOW), 0)
    key_index = lax.broadcasted_iota(jnp.int32, (WINDOW, 2 * WINDOW), 1)
    distance = query_index - key_index + WINDOW
    in_band = (distance >= 0) & (distance < WINDOW)
    block_index = lax.broadcasted_iota(jnp.int32, (block_count, WINDOW, 2 * WINDOW), 0)
    key_position = (
        lax.axis_index("sp") * row_count + block_index * WINDOW - WINDOW + key_index[None]
    )
    allowed = (in_band[None] & (key_position >= 0))[:, None, None]
    scores = jnp.where(allowed, scores, MASKED)
    sink_logit = sinks.reshape(1, kv_local, group_size, 1, 1)
    ceiling = jnp.maximum(jnp.max(scores, axis=-1, keepdims=True), sink_logit)
    weights = jnp.exp(scores - ceiling)
    partition = jnp.exp(sink_logit - ceiling) + jnp.sum(weights, axis=-1, keepdims=True)
    log_total = (
        (ceiling + jnp.log(partition))[..., 0]
        .transpose(0, 3, 1, 2)
        .reshape(row_count, kv_local * group_size)
    )
    probs = (weights / partition).astype(jnp.bfloat16)
    head_out = jnp.einsum(
        "nhgqk,nkhd->nqhgd", probs, value_window, preferred_element_type=jnp.float32
    )
    return (head_out.astype(jnp.bfloat16).reshape(row_count, kv_local * group_size * HD), log_total)


def memory(mem_query, mem_key, mem_value, mem_gate, gate_pre, forget_bias, forget_shift):
    row_count = mem_query.shape[0]
    head_count = forget_bias.shape[0]
    block_count = row_count // BLK
    sequence_total = row_count * lax.axis_size("sp")

    def blocks(array):
        return (
            array.astype(jnp.float32)
            .reshape(block_count, BLK, head_count, HD)
            .transpose(0, 2, 1, 3)
        )

    def gate_blocks(array):
        return array.reshape(block_count, BLK, head_count).transpose(0, 2, 1)

    log_in = gate_pre[:, 0, :] - 0.5 * math.log(sequence_total)
    log_forget = jax.nn.log_sigmoid(gate_pre[:, 1, :] + forget_bias) + forget_shift
    query_blocks = blocks(mem_query)
    key_blocks = blocks(mem_key) * HD ** (-0.5)
    value_blocks = blocks(mem_value)
    in_blocks = gate_blocks(log_in)
    forget_blocks = gate_blocks(log_forget)
    initial = (
        jnp.zeros((head_count, HD, HD), jnp.float32),
        jnp.zeros((head_count, HD), jnp.float32),
        jnp.full((head_count,), MASKED, jnp.float32),
    )

    def summarize(carried, block_data):
        key_block, value_block, in_block, forget_block = block_data
        return (
            advance(carried, key_block, value_block, in_block, jnp.cumsum(forget_block, axis=-1)),
            None,
        )

    summary, _ = lax.scan(summarize, initial, (key_blocks, value_blocks, in_blocks, forget_blocks))
    passed = jnp.sum(log_forget, axis=0)
    identity = (jnp.zeros((head_count,), jnp.float32), initial[0], initial[1], initial[2])
    incoming = entering((passed, summary[0], summary[1], summary[2]), "sp", join_states, identity)
    _, recall = lax.scan(
        block_step,
        (incoming[1], incoming[2], incoming[3]),
        (query_blocks, key_blocks, value_blocks, in_blocks, forget_blocks),
    )
    recall = recall.transpose(0, 2, 1, 3).reshape(row_count, head_count * HD)
    return (recall * jax.nn.sigmoid(mem_gate.astype(jnp.float32))).astype(jnp.bfloat16)


def shards(
    tokens,
    norm_gain,
    w_query,
    w_key,
    w_value,
    w_mem_query,
    w_mem_key,
    w_mem_value,
    w_mem_gate,
    w_gates,
    sinks,
    forget_bias,
    forget_shift,
    w_out,
):
    normed = normalize(tokens, norm_gain)
    token_rows = lax.all_gather(normed, "tp", axis=0, tiled=True)
    row_count = token_rows.shape[0]
    head_count = forget_bias.shape[0]
    gate_columns = lax.dynamic_slice_in_dim(
        w_gates, lax.axis_index("tp") * head_count, head_count, 2
    ).reshape(w_gates.shape[0], 2 * head_count)
    gate_pre = jnp.dot(token_rows, gate_columns, preferred_element_type=jnp.float32).reshape(
        row_count, 2, head_count
    )
    segments = (
        lax.all_gather(w_query, "sp", axis=0, tiled=True),
        lax.all_gather(w_key, "sp", axis=0, tiled=True),
        lax.all_gather(w_value, "sp", axis=0, tiled=True),
        lax.all_gather(w_mem_query, "sp", axis=0, tiled=True),
        lax.all_gather(w_mem_key, "sp", axis=0, tiled=True),
        lax.all_gather(w_mem_value, "sp", axis=0, tiled=True),
        lax.all_gather(w_mem_gate, "sp", axis=0, tiled=True),
    )
    columns = token_rows
    projected_sums = tuple(
        (jnp.dot(columns, segment, preferred_element_type=jnp.float32) for segment in segments)
    )
    projected = [partial_sum.astype(jnp.bfloat16) for partial_sum in projected_sums]
    attn_out, log_total = attend(projected[0], projected[1], projected[2], sinks)
    mem_parts = projected[3:]
    mem_out = memory(
        mem_parts[0], mem_parts[1], mem_parts[2], mem_parts[3], gate_pre, forget_bias, forget_shift
    )
    head_attn, head_mem = (
        lax.all_gather(attn_out, "tp", axis=1, tiled=True),
        lax.all_gather(mem_out, "tp", axis=1, tiled=True),
    )
    joined = jnp.concatenate([head_attn, head_mem], axis=1)
    columns = joined
    mixed = jnp.dot(
        columns, lax.all_gather(w_out, "sp", axis=0, tiled=True), preferred_element_type=jnp.float32
    )
    return (mixed.astype(jnp.bfloat16), log_total)


def solution(mesh):
    placed = (
        P(("sp", "tp"), None),
        P(),
        P("sp", "tp"),
        P("sp", "tp"),
        P("sp", "tp"),
        P("sp", "tp"),
        P("sp", "tp"),
        P("sp", "tp"),
        P("sp", "tp"),
        P(),
        P("tp"),
        P("tp"),
        P("sp", "tp"),
        P("sp", "tp"),
    )
    return jax.shard_map(
        shards,
        mesh=mesh,
        in_specs=placed,
        out_specs=(P("sp", "tp"), P("sp", "tp")),
        check_vma=False,
    )
```

profile of v0, /device:TPU:0, one launch (start us, length us, event | category | flops | bytes accessed | tf_op | source)
XLA Modules:
  0.0 535.0 jit_solution(10117530372503453236)
XLA Ops:
  8.0 1.4 fusion.49
  9.4 2.3 fusion.51
  16.7 36.5 %all-gather.20.cloned.1.call-done = bf16[4096,128]{1,0:T(8,128)(2,1)} async-done(((bf16[512,128]{1,0:T(8,128)(2,1)}), bf16[4096,128]{1,0:T(8,128)(2,1)}) %all-gather.20.cloned.1.call-update) | async-done | bytes 1048592 | tf_op jit(solution)/shard_map/all_gather | solution.py:225
  53.2 29.4 %all-gather.16.cloned.1.call-done = bf16[384,4096]{1,0:T(8,128)(2,1)} async-done(((bf16[96,4096]{1,0:T(8,128)(2,1)}), bf16[384,4096]{1,0:T(8,128)(2,1)}) %all-gather.16.cloned.1.call-update) | async-done | bytes 3145744 | tf_op jit(solution)/shard_map/all_gather | solution.py:214
  82.5 3.3 convolution_convert_fusion.5
  87.1 3.4 collective-permute-start.1
  90.5 34.5 %all-gather.18.cloned.1.call-done = bf16[4096,128]{1,0:T(8,128)(2,1)} async-done(((bf16[512,128]{1,0:T(8,128)(2,1)}), bf16[4096,128]{1,0:T(8,128)(2,1)}) %all-gather.18.cloned.1.call-update) | async-done | bytes 1048592 | tf_op jit(solution)/shard_map/all_gather | solution.py:226
  125.0 2.2 convolution_convert_fusion.6
  127.2 1.7 reshape.294
  130.3 1.7 copy.59
  132.0 3.1 collective-permute-start
  135.1 1.7 copy.55
  136.8 1.5 pad_maximum_fusion
  138.3 1.7 reshape.293
  139.9 1.7 copy.58
  141.6 1.4 pad_maximum_fusion.1
  143.1 1.7 reshape.291
  144.7 1.7 copy.54
  146.4 52.4 %all-gather.22.cloned.1.call-done = bf16[4096,512]{1,0:T(8,128)(2,1)} async-done(((bf16[512,512]{1,0:T(8,128)(2,1)}), bf16[4096,512]{1,0:T(8,128)(2,1)}) %all-gather.22.cloned.1.call-update) | async-done | bytes 4194320 | tf_op jit(solution)/shard_map/all_gather | solution.py:224
  198.8 4.7 convolution_convert_fusion
  203.6 2.6 reshape.295
  206.2 2.0 fusion.44
  212.6 1.5 reshape.253
  214.1 1.5 dot_general.67
  216.8 1.8 fusion.41
  219.2 29.3 %all-gather.26.cloned.1.call-done = bf16[4096,256]{1,0:T(8,128)(2,1)} async-done(((bf16[512,256]{1,0:T(8,128)(2,1)}), bf16[4096,256]{1,0:T(8,128)(2,1)}) %all-gather.26.cloned.1.call-update) | async-done | bytes 2097168 | tf_op jit(solution)/shard_map/all_gather | solution.py:229
  248.5 3.3 fusion.68
  251.9 1.9 copy.64
  253.8 1.9 reshape.263
  255.7 1.9 copy.66
  257.6 40.6 %all-gather.28.cloned.1.call-done = bf16[4096,256]{1,0:T(8,128)(2,1)} async-done(((bf16[512,256]{1,0:T(8,128)(2,1)}), bf16[4096,256]{1,0:T(8,128)(2,1)}) %all-gather.28.cloned.1.call-update) | async-done | bytes 2097168 | tf_op jit(solution)/shard_map/all_gather | solution.py:228
  298.2 3.3 fusion.67
  301.5 1.9 copy.65
  303.4 1.9 mul.176
  305.4 1.8 copy.67
  307.2 2.0 fusion.94
  309.2 22.4 %while.49 = (s32[]{:T(128)}, f32[4,64,64]{2,1,0:T(8,128)S(1)}, f32[4,64]{1,0:T(4,128)}, f32[4]{0:T(128)}, f32[3,4,128]{2,1,0:T(4,128)}, /*index=5*/f32[3,4,128]{...) while((s32[]{:T(128)}, f32[4,64,64]{2,1,0:T(8,128)S(1)}, ...), condition=%wide.region_7.8_spmd.clone, body=%wide.region_4.7_spmd.clone.sunk | while | flops 25709840 | bytes 552793 | solution.py:184
  313.0 1.3 convolution_add_fusion.6
  320.0 1.3 convolution_add_fusion.6
  322.6 1.3 fusion.169
  327.7 1.3 convolution_add_fusion.6
  330.2 1.4 fusion.169
  333.8 19.3 %all-reduce.2 = (bf16[32]{0:T(256)(128)(2,1)S(1)}, bf16[32]{0:T(256)(128)(2,1)S(1)}) all-reduce(bf16[32]{0:T(256)(128)(2,1)} %copy-done.17, bf16[32]{0:T(256)(128)(2,1)} %copy-done.18), channel_id=2, replica_groups=mesh['sp'=8,'tp'=4] {'sp'}, use_global_device_ids=true, to_apply=%add | all-reduce | flops 64 | bytes 256
  353.9 34.9 %all-gather.2 = bf16[32,64,64]{2,1,0:T(8,128)(2,1)} all-gather(bf16[4,64,64]{2,1,0:T(8,128)(2,1)S(1)} %convert_element_type.114), channel_id=4, replica_groups=mesh['sp'=8,'tp'=4] {'sp'}, dimensions={0}, use_global_device_ids=true | all-gather | bytes 294912 | tf_op jit(solution)/shard_map/all_gather | solution.py:24
  389.4 17.3 %all-gather.4 = bf16[8,4,64]{2,1,0:T(4,128)(2,1)} all-gather(bf16[1,4,64]{2,1,0:T(4,128)(2,1)S(1)} %convert_bitcast_fusion), channel_id=5, replica_groups=mesh['sp'=8,'tp'=4] {'sp'}, dimensions={0}, use_global_device_ids=true | all-gather | bytes 4608 | tf_op jit(solution)/shard_map/all_gather | solution.py:24
  406.8 3.4 fusion.65
  410.3 1.9 copy.68
  412.2 1.9 reshape.264
  414.2 30.8 %while.48 = (s32[]{:T(128)}, f32[4,64,64]{2,1,0:T(8,128)S(1)}, f32[4,64]{1,0:T(4,128)S(1)}, f32[4]{0:T(128)S(1)}, f32[3,4,128,64]{2,3,1,0:T(8,128)}, /*index=5*/...) while((s32[]{:T(128)}, f32[4,64,64]{2,1,0:T(8,128)S(1)}, ...), condition=%wide.region_15.16_spmd, body=%wide.region_10.15_spmd.sunk | while | flops 152689152 | bytes 2546069 | solution.py:188
  417.7 1.6 fusion.160
  419.9 1.9 fusion.163
  421.8 1.3 convolution_add_fusion.5
  428.0 1.6 fusion.160
  430.1 2.0 fusion.163
  432.1 1.3 convolution_add_fusion.5
  438.2 1.6 fusion.160
  440.4 1.9 fusion.163
  442.3 1.3 convolution_add_fusion.5
  444.9 2.2 copy.95
  447.1 2.4 reshape.296
  449.5 2.6 fusion.64
  452.2 8.8 %all_gather.71 = bf16[384,1024]{1,0:T(8,128)(2,1)S(1)} all-gather(bf16[384,256]{1,0:T(8,128)(2,1)S(1)} %fusion.64), channel_id=1, replica_groups=mesh['sp'=8,'tp'=4] {'tp'}, dimensions={1}, use_global_device_ids=true | all-gather | bytes 983040 | tf_op jit(solution)/shard_map/all_gather | solution.py:244
  462.0 59.4 %all-gather.34.cloned.1.call-done = bf16[3072,1024]{1,0:T(8,128)(2,1)} async-done(((bf16[384,1024]{1,0:T(8,128)(2,1)}), bf16[3072,1024]{1,0:T(8,128)(2,1)}) %all-gather.34.cloned.1.call-update) | async-done | bytes 6291472 | tf_op jit(solution)/shard_map/all_gather | solution.py:249
  521.4 6.8 %fusion.53 = bf16[384,1024]{1,0:T(8,128)(2,1)} fusion(bf16[3072,1024]{1,0:T(8,128)(2,1)} %all-gather.34.cloned.1.call-done, bf16[384,1024]{0,1:T(8,128)(2,1)S(1)} %copy.74, bf16[384,2048]{0,1:T(8,128)(2,1)} %all-gather.24.cloned.1.call-done), kind=kOutput, calls=%fused_computation.92 | convolution fusion | flops 2421030912 | bytes 9437184 | tf_op jit(solution)/shard_map/dot_general | solution.py:248
  (166 shorter events, 50.4 us)
Async XLA Ops:
  7.2 204.8 %copy-start = (bf16[4096,2,16]{0,2,1:T(8,128)(2,1)S(1)}, bf16[4096,2,16]{0,2,1:T(8,128)(2,1)}, u32[]{:S(2)}) copy-start(bf16[4096,2,16]{0,2,1:T(8,128)(2,1)} %param.29) | copy-start | bytes 786436
  7.2 8.5 %copy-start.15 = (f32[8]{0:T(128)S(1)}, f32[8]{0:T(128)}, u32[]{:S(2)}) copy-start(f32[8]{0:T(128)} %param.30) | copy-start | bytes 100
  7.2 46.0 %all-gather.20.cloned.1.call-start = ((), (), s32[]{:S(2)}) async-start(), calls=%async_computation.2 | async-start | bytes 1179648 | tf_op jit(solution)/shard_map/all_gather | solution.py:225
  7.9 74.6 %all-gather.16.cloned.1.call-start = ((), (), s32[]{:S(2)}) async-start(), calls=%async_computation | async-start | bytes 3932160 | tf_op jit(solution)/shard_map/all_gather | solution.py:214
  11.7 113.3 %all-gather.18.cloned.1.call-start = ((), (), s32[]{:S(2)}) async-start(), calls=%async_computation.1 | async-start | bytes 1179648 | tf_op jit(solution)/shard_map/all_gather | solution.py:226
  12.4 186.4 %all-gather.22.cloned.1.call-start = ((), (), s32[]{:S(2)}) async-start(), calls=%async_computation.3 | async-start | bytes 4718592 | tf_op jit(solution)/shard_map/all_gather | solution.py:224
  13.0 235.5 %all-gather.26.cloned.1.call-start = ((), (), s32[]{:S(2)}) async-start(), calls=%async_computation.5 | async-start | bytes 2359296 | tf_op jit(solution)/shard_map/all_gather | solution.py:229
  13.6 284.6 %all-gather.28.cloned.1.call-start = ((), (), s32[]{:S(2)}) async-start(), calls=%async_computation.6 | async-start | bytes 2359296 | tf_op jit(solution)/shard_map/all_gather | solution.py:228
  14.2 392.7 %all-gather.30.cloned.1.call-start = ((), (), s32[]{:S(2)}) async-start(), calls=%async_computation.7 | async-start | bytes 2359296 | tf_op jit(solution)/shard_map/all_gather | solution.py:227
  14.9 434.6 %all-gather.32.cloned.1.call-start = ((), (), s32[]{:S(2)}) async-start(), calls=%async_computation.8 | async-start | bytes 2359296 | tf_op jit(solution)/shard_map/all_gather | solution.py:230
  15.7 446.4 %all-gather.24.cloned.1.call-start = ((), (), s32[]{:S(2)}) async-start(), calls=%async_computation.4 | async-start | bytes 1966080 | tf_op jit(solution)/shard_map/all_gather | solution.py:243
  15.8 193.2 %copy-start.12 = (f32[2,4]{1,0:T(2,128)}, f32[2,4]{1,0:T(2,128)S(1)}, u32[]{:S(2)}) copy-start(f32[2,4]{1,0:T(2,128)S(1)} %max.59) | copy-start | bytes 100
  82.5 42.4 %copy-start.1 = (bf16[384,4096]{1,0:T(8,128)(2,1)S(1)}, bf16[384,4096]{1,0:T(8,128)(2,1)}, u32[]{:S(2)}) copy-start(bf16[384,4096]{1,0:T(8,128)(2,1)} %all-gather.16.cloned.1.call-done) | copy-start | bytes 9437188
  85.8 0.6 copy-start.2
  87.1 49.7 %collective-permute-start.1 = (bf16[128,128]{1,0:T(8,128)(2,1)}, bf16[128,128]{1,0:T(8,128)(2,1)S(1)}, u32[]{:S(2)}, u32[]{:S(2)}) collective-permute-start(bf16[128,128]{1,0:T(8,128)(2,1)} %slice.50), channel_id=1, source_target_pairs={{0,4},{4,8},{8,12},{12,16},{16,20},{20,24},{24,28},{1,5},{5,9},{9,... | collective-permute-start | bytes 98312 | tf_op jit(solution)/shard_map/ppermute | solution.py:18
  132.0 9.6 %collective-permute-start = (bf16[128,128]{1,0:T(8,128)(2,1)}, bf16[128,128]{1,0:T(8,128)(2,1)}, u32[]{:S(2)}, u32[]{:S(2)}) collective-permute-start(bf16[128,128]{1,0:T(8,128)(2,1)} %slice.49), channel_id=1, source_target_pairs={{0,4},{4,8},{8,12},{12,16},{16,20},{20,24},{24,28},{1,5},{5,9},{9,... | collective-permute-start | bytes 98312 | tf_op jit(solution)/shard_map/ppermute | solution.py:18
  146.4 59.8 %copy-start.3 = (pred[3,128,256]{1,2,0:T(8,128)(4,1)S(1)}, pred[3,128,256]{1,2,0:T(8,128)(4,1)}, u32[]{:S(2)}) copy-start(pred[3,128,256]{1,2,0:T(8,128)(4,1)} %fusion.71) | copy-start | bytes 294916
  206.2 2.9 copy-start.9
  206.2 2.9 copy-start.10
  208.3 1.8 copy-start.7
  209.0 1.1 copy-start.5
  210.1 5.5 %copy-start.16 = (u32[32]{0:T(128)S(1)}, u32[32]{0:T(128)}, u32[]{:S(2)}) copy-start(u32[32]{0:T(128)} %constant.110) | copy-start | bytes 388
  211.3 310.1 %all-gather.34.cloned.1.call-start = ((), (), s32[]{:S(2)}) async-start(), calls=%async_computation.9 | async-start | bytes 7077888 | tf_op jit(solution)/shard_map/all_gather | solution.py:249
  218.6 0.6 copy-start.11
  257.6 49.6 %copy-start.14 = (f32[4]{0:T(128)S(1)}, f32[4]{0:T(128)}, u32[]{:S(2)}) copy-start(f32[4]{0:T(128)} %param.31) | copy-start | bytes 52
  331.6 75.2 %copy-start.4 = (f32[3,4,128]{2,1,0:T(4,128)}, f32[3,4,128]{2,1,0:T(4,128)S(1)}, u32[]{:S(2)}) copy-start(f32[3,4,128]{2,1,0:T(4,128)S(1)} %get-tuple-element.643) | copy-start | bytes 18436
  332.4 0.9 copy-start.18
  333.3 0.5 copy-start.17
  449.5 11.8 %copy-start.6 = (f32[3,2,4,128]{3,2,1,0:T(4,128)S(1)}, f32[3,2,4,128]{3,2,1,0:T(4,128)}, u32[]{:S(2)}) copy-start(f32[3,2,4,128]{3,2,1,0:T(4,128)} %copy-done.5) | copy-start | bytes 36868
  449.5 11.8 %copy-start.8 = (f32[3,2,4,128]{3,2,1,0:T(4,128)S(1)}, f32[3,2,4,128]{3,2,1,0:T(4,128)}, u32[]{:S(2)}) copy-start(f32[3,2,4,128]{3,2,1,0:T(4,128)} %copy-done.7) | copy-start | bytes 36868
  449.5 11.8 %copy-start.13 = (f32[2,4]{1,0:T(2,128)S(1)}, f32[2,4]{1,0:T(2,128)}, u32[]{:S(2)}) copy-start(f32[2,4]{1,0:T(2,128)} %copy-done.12) | copy-start | bytes 100
Sparse Core Ops, SparseCore 0:
  10.1 42.9 all-gather.19
  55.3 27.2 all-gather.15
  84.7 40.2 all-gather.17
  127.0 71.8 all-gather.21
  200.8 47.6 all-gather.25
  250.5 47.6 all-gather.27
  300.3 47.9 all-gather.29
  350.4 49.6 all-gather.31
  401.6 18.9 all-gather.23
  422.6 98.7 all-gather.33
where the time goes:
time: 538 us; the launch traced here: 535 us
  waiting for transfers between devices  287 us (53%)
  blocking collectives  80.3 us (15%)
  matrix products  61.6 us (11%)
  local copies, waits for them, and re-layouts  54.6 us (10%)
  other arithmetic  29.4 us (5%)
  between operations  15.1 us (3%)
  starting transfers between devices  7 us (1%)
    all_gather x1, waiting for transfers between devices, shards(): lax.all_gather(w_out, 'sp', axis=0, tiled=True)  59.4 us
    all_gather x1, waiting for transfers between devices, shards(): lax.all_gather(w_query, 'sp', axis=0, tiled=True)  52.4 us
    all_gather x2, blocking collectives, entering(): lax.all_gather(a.astype(kind), axis)  52.2 us
    all_gather x1, waiting for transfers between devices, shards(): lax.all_gather(w_mem_key, 'sp', axis=0, tiled=True)  40.6 us
    all_gather x1, waiting for transfers between devices, shards(): lax.all_gather(w_key, 'sp', axis=0, tiled=True)  36.5 us
    all_gather x1, waiting for transfers between devices, shards(): lax.all_gather(w_value, 'sp', axis=0, tiled=True)  34.5 us
    all_gather x1, waiting for transfers between devices, shards(): token_rows = lax.all_gather(normed, 'tp', axis=0, tiled=True)  29.4 us
    all_gather x1, waiting for transfers between devices, shards(): lax.all_gather(w_mem_value, 'sp', axis=0, tiled=True)  29.3 us
  transfers between devices with their start and end apart: 12, of which 7 were waited for; matrix products, arithmetic and copies ran while one was open for 26% of the time, Pallas kernels for 0%

commit v1 on v0

--- a/solution.py
+++ b/solution.py
@@ -211,7 +211,13 @@
     w_out,
 ):
     normed = normalize(tokens, norm_gain)
-    token_rows = lax.all_gather(normed, "tp", axis=0, tiled=True)
+    peers = lax.axis_size("tp")
+    held, pieces = (normed, [normed])
+    for _ in range(peers - 1):
+        held = lax.ppermute(held, "tp", [(i_2, (i_2 + 1) % peers) for i_2 in range(peers)])
+        pieces.insert(0, held)
+    row_of_blocks = jnp.concatenate(pieces, axis=0)
+    token_rows = jnp.roll(row_of_blocks, (lax.axis_index("tp") + 1) * normed.shape[0], axis=0)
     row_count = token_rows.shape[0]
     head_count = forget_bias.shape[0]
     gate_columns = lax.dynamic_slice_in_dim(

time: 538 us -> 505 us (0.939)
  waiting for transfers between devices: 287 us -> 331 us
  local copies, waits for them, and re-layouts: 54.6 us -> 13.6 us
  other arithmetic: 29.4 us -> 12.2 us
  matrix products: 61.6 us -> 45.3 us
    all_gather x1, waiting for transfers between devices: 59.4 us -> 99.8 us  [shards(): lax.all_gather(w_out, 'sp', axis=0, tiled=True)]
    all_gather x1, waiting for transfers between devices: 36.5 us -> 0.01 us  [shards(): lax.all_gather(w_key, 'sp', axis=0, tiled=True)]
    ppermute x0 -> x3, waiting for transfers between devices: none -> 34 us  [shards(): lax.ppermute(held, 'tp', [(i_2, (i_2 + 1) % peers) for i_2 in range(peers)])]
    all_gather x1 -> x0, waiting for transfers between devices: 29.4 us -> none  [shards(): token_rows = lax.all_gather(normed, 'tp', axis=0, tiled=True)]
    all_gather x1, waiting for transfers between devices: 52.4 us -> 65.7 us  [shards(): lax.all_gather(w_query, 'sp', axis=0, tiled=True)]
    all_gather x1, waiting for transfers between devices: 0.01 us -> 9.8 us  [shards(): lax.all_gather(w_mem_gate, 'sp', axis=0, tiled=True)]
    transpose x4, local copies, waits for them, and re-layouts: 7.74 us -> 0.64 us  [blocks(): return array.astype(jnp.float32).reshape(block_count, BLK, head_count, HD...]
    slice x4, local copies, waits for them, and re-layouts: 6.76 us -> 0.52 us  [attend(): key_window = jnp.concatenate([padded_keys[:-1], padded_keys[1:]], axis=1)]
  transfers between devices with their start and end apart: 12 -> 14, of which waited for: 7 -> 11; matrix products, arithmetic and copies ran while one was open for 26% -> 13% of each run, Pallas kernels for 0% -> 0%
where the time goes in v1:
time: 505 us
  waiting for transfers between devices  331 us (66%)
  blocking collectives  79.3 us (16%)
  matrix products  45.3 us (9%)
  between operations  15 us (3%)
  local copies, waits for them, and re-layouts  13.6 us (3%)
  other arithmetic  12.2 us (2%)
  starting transfers between devices  7.8 us (2%)
    all_gather x1, waiting for transfers between devices, shards(): lax.all_gather(w_out, 'sp', axis=0, tiled=True)  99.8 us
    all_gather x1, waiting for transfers between devices, shards(): lax.all_gather(w_query, 'sp', axis=0, tiled=True)  65.7 us
    all_gather x2, blocking collectives, entering(): lax.all_gather(a.astype(kind), axis)  51.2 us
    all_gather x1, waiting for transfers between devices, shards(): lax.all_gather(w_mem_key, 'sp', axis=0, tiled=True)  45.7 us
    all_gather x1, waiting for transfers between devices, shards(): lax.all_gather(w_mem_value, 'sp', axis=0, tiled=True)  35.1 us
    ppermute x3, waiting for transfers between devices, shards(): lax.ppermute(held, 'tp', [(i_2, (i_2 + 1) % peers) for i_2 in range(peers)])  34 us
    all_gather x1, waiting for transfers between devices, shards(): lax.all_gather(w_value, 'sp', axis=0, tiled=True)  29.7 us
    dot_general x7, matrix products, shards(): jnp.dot(columns, segment, preferred_element_type=jnp.float32)  25.5 us
  transfers between devices with their start and end apart: 14, of which 11 were waited for; matrix products, arithmetic and copies ran while one was open for 13% of the time, Pallas kernels for 0%

profile of v1, /device:TPU:0, one launch (start us, length us, event | category | flops | bytes accessed | tf_op | source)
XLA Modules:
  0.0 505.0 jit_solution(6668782783983865761)
XLA Ops:
  7.2 0.7 all-gather.17.cloned.1.call-update
  8.0 0.7 all-gather.15.cloned.1.call-update
  8.7 0.7 all-gather.19.cloned.1.call-update
  9.5 0.5 all-gather.23.cloned.1.call-update
  10.0 0.5 all-gather.25.cloned.1.call-update
  10.6 0.5 all-gather.27.cloned.1.call-update
  11.2 1.4 fusion.49
  12.6 1.5 fusion.51
  14.1 0.5 collective-permute-start
  14.6 11.6 %collective-permute-done = bf16[96,4096]{1,0:T(8,128)(2,1)S(1)} collective-permute-done((bf16[96,4096]{1,0:T(8,128)(2,1)S(1)}, bf16[96,4096]{1,0:T(8,128)(2,1)S(1)}, u32[]{:S(2)}, u32[]{:S(2)}) %collective-permute-start) | collective-permute-done | bytes 786464 | tf_op jit(solution)/shard_map/ppermute | solution.py:217
  26.2 11.4 %collective-permute-done.1 = bf16[96,4096]{1,0:T(8,128)(2,1)S(1)} collective-permute-done((bf16[96,4096]{1,0:T(8,128)(2,1)S(1)}, bf16[96,4096]{1,0:T(8,128)(2,1)S(1)}, u32[]{:S(2)}, u32[]{:S(2)}) %collective-permute-start.1) | collective-permute-done | bytes 786464 | tf_op jit(solution)/shard_map/ppermute | solution.py:217
  38.0 11.0 %collective-permute-done.2 = bf16[96,4096]{1,0:T(8,128)(2,1)S(1)} collective-permute-done((bf16[96,4096]{1,0:T(8,128)(2,1)S(1)}, bf16[96,4096]{1,0:T(8,128)(2,1)S(1)}, u32[]{:S(2)}, u32[]{:S(2)}) %collective-permute-start.2) | collective-permute-done | bytes 786464 | tf_op jit(solution)/shard_map/ppermute | solution.py:217
  49.1 1.0 constant_dynamic-update-slice_fusion.7
  50.0 0.9 constant_dynamic-update-slice_fusion.6
  51.0 1.0 constant_dynamic-update-slice_fusion.5
  52.0 1.2 constant_dynamic-update-slice_fusion.4
  53.2 0.9 constant_dynamic-update-slice_fusion.3
  54.2 1.0 constant_dynamic-update-slice_fusion.2
  55.1 0.9 constant_dynamic-update-slice_fusion.1
  56.1 1.2 constant_dynamic-update-slice_fusion
  57.2 3.2 convolution_convert_fusion.5
  60.4 4.2 collective-permute-start.4
  64.7 29.7 %all-gather.15.cloned.1.call-done = bf16[4096,128]{1,0:T(8,128)(2,1)} async-done(((bf16[512,128]{1,0:T(8,128)(2,1)}), bf16[4096,128]{1,0:T(8,128)(2,1)}) %all-gather.15.cloned.1.call-update) | async-done | bytes 1048592 | tf_op jit(solution)/shard_map/all_gather | solution.py:232
  94.4 3.2 convolution_convert_fusion.6
  98.0 2.5 collective-permute-start.3
  100.9 1.1 collective-permute-done.3
  102.3 65.7 %all-gather.19.cloned.1.call-done = bf16[4096,512]{1,0:T(8,128)(2,1)} async-done(((bf16[512,512]{1,0:T(8,128)(2,1)}), bf16[4096,512]{1,0:T(8,128)(2,1)}) %all-gather.19.cloned.1.call-update) | async-done | bytes 4194320 | tf_op jit(solution)/shard_map/all_gather | solution.py:230
  168.1 5.0 convolution_convert_fusion
  173.0 0.4 reshape.295
  173.4 0.7 fusion.44
  174.2 0.7 fusion.43
  175.0 0.9 fusion.57
  176.3 0.8 copy.104
  177.4 0.5 all-gather.31.cloned.1.call-update
  178.1 0.6 dynamic-slice
  179.3 2.8 fusion.41
  182.6 35.1 %all-gather.23.cloned.1.call-done = bf16[4096,256]{1,0:T(8,128)(2,1)} async-done(((bf16[512,256]{1,0:T(8,128)(2,1)}), bf16[4096,256]{1,0:T(8,128)(2,1)}) %all-gather.23.cloned.1.call-update) | async-done | bytes 2097168 | tf_op jit(solution)/shard_map/all_gather | solution.py:235
  217.8 3.5 fusion.68
  221.7 45.7 %all-gather.25.cloned.1.call-done = bf16[4096,256]{1,0:T(8,128)(2,1)} async-done(((bf16[512,256]{1,0:T(8,128)(2,1)}), bf16[4096,256]{1,0:T(8,128)(2,1)}) %all-gather.25.cloned.1.call-update) | async-done | bytes 2097168 | tf_op jit(solution)/shard_map/all_gather | solution.py:234
  267.4 3.5 fusion.67
  271.3 4.6 while.49
  276.0 32.9 %all-gather.2 = bf16[32,64,64]{2,1,0:T(8,128)(2,1)S(1)} all-gather(bf16[4,64,64]{2,1,0:T(8,128)(2,1)S(1)} %convert_element_type.114), channel_id=4, replica_groups=mesh['sp'=8,'tp'=4] {'sp'}, dimensions={0}, use_global_device_ids=true | all-gather | bytes 294912 | tf_op jit(solution)/shard_map/all_gather | solution.py:24
  309.1 18.3 %all-gather.4 = bf16[8,4,64]{2,1,0:T(4,128)(2,1)S(1)} all-gather(bf16[1,4,64]{2,1,0:T(4,128)(2,1)S(1)} %convert_bitcast_fusion), channel_id=5, replica_groups=mesh['sp'=8,'tp'=4] {'sp'}, dimensions={0}, use_global_device_ids=true | all-gather | bytes 4608 | tf_op jit(solution)/shard_map/all_gather | solution.py:24
  327.5 17.6 %all-reduce.2 = (bf16[32]{0:T(256)(128)(2,1)S(1)}, bf16[32]{0:T(256)(128)(2,1)S(1)}) all-reduce(bf16[32]{0:T(256)(128)(2,1)S(1)} %dynamic-update-slice, bf16[32]{0:T(256)(128)(2,1)S(1)} %dynamic-update-slice.1), channel_id=2, replica_groups=mesh['sp'=8,'tp'=4] {'sp'}, use_global_device_ids=true, to_apply=%add | all-reduce | flops 64 | bytes 256
  345.3 3.6 fusion.65
  349.2 10.6 %while.48 = (s32[]{:T(128)}, f32[4,64,64]{2,1,0:T(8,128)S(1)}, f32[4,64]{1,0:T(4,128)S(1)}, f32[4]{0:T(128)S(1)}, f32[3,4,128,64]{2,3,1,0:T(8,128)S(1)}, /*index...) while((s32[]{:T(128)}, f32[4,64,64]{2,1,0:T(8,128)S(1)}, ...), condition=%wide.region_15.16_spmd, body=%wide.region_10.15_spmd.sunk | while | flops 152689152 | bytes 2611085 | solution.py:188
  350.3 0.7 fusion.169
  351.6 0.4 fusion.172
  352.0 0.3 convolution_add_fusion.5
  353.9 0.7 fusion.169
  355.1 0.4 fusion.172
  355.5 0.3 convolution_add_fusion.5
  357.4 0.7 fusion.169
  358.7 0.4 fusion.172
  359.0 0.3 convolution_add_fusion.5
  360.1 0.5 reshape.296
  360.6 9.8 %all-gather.29.cloned.1.call-done = bf16[4096,256]{1,0:T(8,128)(2,1)} async-done(((bf16[512,256]{1,0:T(8,128)(2,1)}), bf16[4096,256]{1,0:T(8,128)(2,1)}) %all-gather.29.cloned.1.call-update) | async-done | bytes 2097168 | tf_op jit(solution)/shard_map/all_gather | solution.py:236
  370.4 3.6 fusion.64
  374.0 10.6 %all_gather.67 = bf16[384,1024]{1,0:T(8,128)(2,1)S(1)} all-gather(bf16[384,256]{1,0:T(8,128)(2,1)S(1)} %fusion.64), channel_id=1, replica_groups=mesh['sp'=8,'tp'=4] {'tp'}, dimensions={1}, use_global_device_ids=true | all-gather | bytes 983040 | tf_op jit(solution)/shard_map/all_gather | solution.py:250
  384.5 0.4 copy.74
  384.9 0.7 fusion.88
  385.6 6.2 %all-gather.21.cloned.1.call-done = bf16[384,2048]{0,1:T(8,128)(2,1)} async-done(((bf16[384,512]{0,1:T(8,128)(2,1)}), bf16[384,2048]{0,1:T(8,128)(2,1)}) %all-gather.21.cloned.1.call-update) | async-done | bytes 1572880 | tf_op jit(solution)/shard_map/all_gather | solution.py:249
  391.8 99.8 %all-gather.31.cloned.1.call-done = bf16[3072,1024]{1,0:T(8,128)(2,1)} async-done(((bf16[384,1024]{1,0:T(8,128)(2,1)}), bf16[3072,1024]{1,0:T(8,128)(2,1)}) %all-gather.31.cloned.1.call-update) | async-done | bytes 6291472 | tf_op jit(solution)/shard_map/all_gather | solution.py:255
  491.6 6.8 %fusion.53 = bf16[384,1024]{1,0:T(8,128)(2,1)} fusion(bf16[3072,1024]{1,0:T(8,128)(2,1)} %all-gather.31.cloned.1.call-done, bf16[384,1024]{0,1:T(8,128)(2,1)S(1)} %copy.74, bf16[384,2048]{0,1:T(8,128)(2,1)} %all-gather.21.cloned.1.call-done), kind=kOutput, calls=%fused_computation.92 | convolution fusion | flops 2421030912 | bytes 9437184 | tf_op jit(solution)/shard_map/dot_general | solution.py:254
  (153 shorter events, 15.8 us)
Async XLA Ops:
  7.2 170.8 %copy-start = (bf16[4096,2,16]{0,2,1:T(8,128)(2,1)S(1)}, bf16[4096,2,16]{0,2,1:T(8,128)(2,1)}, u32[]{:S(2)}) copy-start(bf16[4096,2,16]{0,2,1:T(8,128)(2,1)} %param.29) | copy-start | bytes 786436
  7.2 30.6 %copy-start.5 = (f32[8]{0:T(128)S(1)}, f32[8]{0:T(128)}, u32[]{:S(2)}) copy-start(f32[8]{0:T(128)} %param.30) | copy-start | bytes 100
  7.2 50.0 %all-gather.17.cloned.1.call-start = ((), (), s32[]{:S(2)}) async-start(), calls=%async_computation.1 | async-start | bytes 1179648 | tf_op jit(solution)/shard_map/all_gather | solution.py:231
  7.9 86.5 %all-gather.15.cloned.1.call-start = ((), (), s32[]{:S(2)}) async-start(), calls=%async_computation | async-start | bytes 1179648 | tf_op jit(solution)/shard_map/all_gather | solution.py:232
  8.7 159.4 %all-gather.19.cloned.1.call-start = ((), (), s32[]{:S(2)}) async-start(), calls=%async_computation.2 | async-start | bytes 4718592 | tf_op jit(solution)/shard_map/all_gather | solution.py:230
  9.4 208.4 %all-gather.23.cloned.1.call-start = ((), (), s32[]{:S(2)}) async-start(), calls=%async_computation.4 | async-start | bytes 2359296 | tf_op jit(solution)/shard_map/all_gather | solution.py:235
  10.0 257.4 %all-gather.25.cloned.1.call-start = ((), (), s32[]{:S(2)}) async-start(), calls=%async_computation.5 | async-start | bytes 2359296 | tf_op jit(solution)/shard_map/all_gather | solution.py:234
  10.6 334.7 %all-gather.27.cloned.1.call-start = ((), (), s32[]{:S(2)}) async-start(), calls=%async_computation.6 | async-start | bytes 2359296 | tf_op jit(solution)/shard_map/all_gather | solution.py:233
  11.1 359.3 %all-gather.29.cloned.1.call-start = ((), (), s32[]{:S(2)}) async-start(), calls=%async_computation.7 | async-start | bytes 2359296 | tf_op jit(solution)/shard_map/all_gather | solution.py:236
  12.6 39.4 %copy-start.1 = (bf16[96,4096]{1,0:T(8,128)(2,1)S(1)}, bf16[96,4096]{1,0:T(8,128)(2,1)}, u32[]{:S(2)}) copy-start(bf16[96,4096]{1,0:T(8,128)(2,1)} %param.20) | copy-start | bytes 2359300
  12.6 39.4 %copy-start.2 = (f32[4096]{0:T(1024)S(1)}, f32[4096]{0:T(1024)}, u32[]{:S(2)}) copy-start(f32[4096]{0:T(1024)} %param.21) | copy-start | bytes 49156
  14.1 12.1 %collective-permute-start = (bf16[96,4096]{1,0:T(8,128)(2,1)S(1)}, bf16[96,4096]{1,0:T(8,128)(2,1)S(1)}, u32[]{:S(2)}, u32[]{:S(2)}) collective-permute-start(bf16[96,4096]{1,0:T(8,128)(2,1)S(1)} %fusion.51), channel_id=1, source_target_pairs={{0,1},{1,2},{2,3},{3,0},{4,5},{5,6},{6,7},{7,4},{8,9},{9,10},{10,1... | collective-permute-start | bytes 2359304 | tf_op jit(solution)/shard_map/ppermute | solution.py:217
  26.2 11.4 %collective-permute-start.1 = (bf16[96,4096]{1,0:T(8,128)(2,1)S(1)}, bf16[96,4096]{1,0:T(8,128)(2,1)S(1)}, u32[]{:S(2)}, u32[]{:S(2)}) collective-permute-start(bf16[96,4096]{1,0:T(8,128)(2,1)S(1)} %collective-permute-done), channel_id=1, source_target_pairs={{0,1},{1,2},{2,3},{3,0},{4,5},{5,6},{6,7},{7,4},{8,9},{9,10},{10,1... | collective-permute-start | bytes 2359304 | tf_op jit(solution)/shard_map/ppermute | solution.py:217
  37.6 11.4 %collective-permute-start.2 = (bf16[96,4096]{1,0:T(8,128)(2,1)S(1)}, bf16[96,4096]{1,0:T(8,128)(2,1)S(1)}, u32[]{:S(2)}, u32[]{:S(2)}) collective-permute-start(bf16[96,4096]{1,0:T(8,128)(2,1)S(1)} %collective-permute-done.1), channel_id=1, source_target_pairs={{0,1},{1,2},{2,3},{3,0},{4,5},{5,6},{6,7},{7,4},{8,9},{9,10},{10,1... | collective-permute-start | bytes 2359304 | tf_op jit(solution)/shard_map/ppermute | solution.py:217
  37.7 354.1 %all-gather.21.cloned.1.call-start = ((), (), s32[]{:S(2)}) async-start(), calls=%async_computation.3 | async-start | bytes 1966080 | tf_op jit(solution)/shard_map/all_gather | solution.py:249
  60.4 40.2 %collective-permute-start.4 = (bf16[128,128]{1,0:T(8,128)(2,1)S(1)}, bf16[128,128]{1,0:T(8,128)(2,1)S(1)}, u32[]{:S(2)}, u32[]{:S(2)}) collective-permute-start(bf16[128,128]{1,0:T(8,128)(2,1)S(1)} %slice.50), channel_id=1, source_target_pairs={{0,4},{4,8},{8,12},{12,16},{16,20},{20,24},{24,28},{1,5},{5,9},{9,... | collective-permute-start | bytes 98312 | tf_op jit(solution)/shard_map/ppermute | solution.py:18
  98.0 4.1 collective-permute-start.3
  175.9 2.1 copy-start.6
  175.9 6.2 %copy-start.3 = (f32[384,4]{0,1:T(4,128)S(1)}, f32[384,4]{0,1:T(4,128)}, u32[]{:S(2)}) copy-start(f32[384,4]{0,1:T(4,128)} %param.32) | copy-start | bytes 18436
  176.0 6.2 %copy-start.4 = (f32[4]{0:T(128)S(1)}, f32[4]{0:T(128)}, u32[]{:S(2)}) copy-start(f32[4]{0:T(128)} %param.31) | copy-start | bytes 52
  177.1 314.5 %all-gather.31.cloned.1.call-start = ((), (), s32[]{:S(2)}) async-start(), calls=%async_computation.8 | async-start | bytes 7077888 | tf_op jit(solution)/shard_map/all_gather | solution.py:255
Sparse Core Ops, SparseCore 0:
  10.1 42.9 all-gather.16
  55.3 39.0 all-gather.14
  96.5 71.4 all-gather.18
  170.0 47.6 all-gather.22
  219.7 47.6 all-gather.24
  269.4 49.8 all-gather.26
  321.4 48.9 all-gather.28
  372.5 19.2 all-gather.20
  394.0 97.6 all-gather.30
